TPU v7x, 32 devices: a whole 2x2x4 slice. The times are simulated.
32 devices in a mesh: grp: 2 (over x), ra: 4 (over y, core), cb: 4 (over z).
Axes of the slice: x: 2, y: 2, z: 4, core: 2. Of those that a mesh axis runs over, the one named last changes fastest.
Arguments:
- tokens: bfloat16 [256, 4096], P('grp', 'ra'), parts along dimension 0, may hold values from -400 to 400
- gain_first: float32 [4096], P('ra'), may hold values from 0.1 to 1.9
- up_first: bfloat16 [4096, 16384], P('ra', 'cb'), may hold values from -0.09375 to 0.09375
- down_first: bfloat16 [16384, 4096], P('cb', 'ra'), may hold values from -2 to 2
- gain_second: float32 [4096], P('ra'), may hold values from 0.1 to 1.9
- up_second: bfloat16 [4096, 16384], P('ra', 'cb'), may hold values from -0.09375 to 0.09375
- down_second: bfloat16 [16384, 4096], P('cb', 'ra'), may hold values from -2 to 2
- gain_last: float32 [4096], P('ra'), may hold values from 0.1 to 1.9
Outputs:
- normed_out: bfloat16 [256, 4096], P('grp', 'ra'), parts along dimension 0
There are 2 independent parts, one for each index of `grp`. A program takes and returns all parts, laid end to end along the dimension named above; an argument that names none is the same for every part. Nothing has to cross between parts.
All inputs are finite; a program needn't handle non-finite values.
Results may differ from a plain program's by a relative error of at most 0.0081.
Values may be sent and summed in bfloat16 or wider, within the bound.
A program may use at most 64 MiB of HBM per device.

v0:
```python
import jax
import jax.numpy as jnp
from jax import lax
from jax.sharding import PartitionSpec as P

D = 4096


norm_eps = 1e-06
residual_keep = 0.5


def mlp_block(stream, gain, up_weight, down_weight):
    squares = jnp.sum(stream * stream, axis=1, keepdims=True)
    normed = (stream * gain).astype(jnp.bfloat16)
    partial_value = jnp.dot(normed, up_weight, preferred_element_type=jnp.float32)
    squares_all = lax.psum(squares, "ra")
    row_scale = lax.rsqrt(squares_all / D + norm_eps)
    share = lax.psum_scatter(partial_value, "ra", scatter_dimension=1, tiled=True)
    activated = jnp.square(jax.nn.relu(share * row_scale)).astype(jnp.bfloat16)
    hidden = lax.all_gather(activated, "ra", axis=1, tiled=True)
    branch_out = jnp.dot(hidden, down_weight, preferred_element_type=jnp.float32)
    branch_out = lax.psum(branch_out, "cb")
    return residual_keep * stream + branch_out


def per_device(
    tokens, gain_first, up_first, down_first, gain_second, up_second, down_second, gain_last
):
    stream = tokens.astype(jnp.float32)
    stream = mlp_block(stream, gain_first, up_first, down_first)
    stream = mlp_block(stream, gain_second, up_second, down_second)
    squares_all = lax.psum(jnp.sum(stream * stream, axis=1, keepdims=True), "ra")
    row_scale = lax.rsqrt(squares_all / D + norm_eps)
    return (stream * row_scale * gain_last).astype(jnp.bfloat16)


def solution(mesh):
    in_specs = (
        P("grp", "ra"),
        P("ra"),
        P("ra", "cb"),
        P("cb", "ra"),
        P("ra"),
        P("ra", "cb"),
        P("cb", "ra"),
        P("ra"),
    )
    out_specs = P("grp", "ra")
    return jax.shard_map(
        per_device, mesh=mesh, in_specs=in_specs, out_specs=out_specs, check_vma=False
    )
```

profile of v0, /device:TPU:0, one launch (start us, length us, event | category | flops | bytes accessed | tf_op | source)
XLA Modules:
  0.0 226.4 jit_solution(142977622871366743)
XLA Ops:
  6.5 6.1 %fusion.4 = f32[128,4096]{1,0:T(8,128)} fusion(bf16[1024,4096]{1,0:T(8,128)(2,1)} %param.10, bf16[128,1024]{1,0:T(8,128)(2,1)} %param.8, f32[1024]{0:T(1024)} %param.9), kind=kOutput, calls=%fused_computation.14 | convolution fusion | flops 1074135040 | bytes 10752000 | tf_op jit(solution)/shard_map/dot_general | solution.py:16
  12.7 0.0 reduce-scatter.3.cloned.1.call-update
  12.7 0.0 all-gather.3.cloned.1.call-start
  12.8 0.1 fusion.2
  12.9 8.4 %psum.35 = f32[128,1]{0,1:T(1,128)S(1)} all-reduce(f32[128,1]{0,1:T(1,128)S(1)} %bitcast.15), channel_id=1, replica_groups=mesh['grp'=2,'ra'=4,'cb'=4] {'ra'}, use_global_device_ids=true, to_apply=%region_2.0 | all-reduce | flops 128 | bytes 1024 | tf_op jit(solution)/shard_map/psum | solution.py:17
  21.3 25.5 %reduce-scatter.3.cloned.1.call-done = f32[128,1024]{1,0:T(8,128)} async-done(((f32[128,4096]{1,0:T(8,128)}), f32[128,1024]{1,0:T(8,128)}) %reduce-scatter.3.cloned.1.call-update) | async-done | bytes 524304 | tf_op jit(solution)/shard_map/reduce_scatter | solution.py:19
  46.8 1.9 multiply_convert_fusion.3
  48.7 0.0 all-gather.3.cloned.1.call-update
  48.7 0.0 copy-start.2
  48.7 0.0 all-reduce.3.cloned.1.call-start
  48.7 16.8 %all-gather.3.cloned.1.call-done = bf16[128,4096]{1,0:T(8,128)(2,1)} async-done(((bf16[128,1024]{1,0:T(8,128)(2,1)}), bf16[128,4096]{1,0:T(8,128)(2,1)}) %all-gather.3.cloned.1.call-update) | async-done | bytes 1048592 | tf_op jit(solution)/shard_map/all_gather | solution.py:21
  65.5 5.8 %fusion.9 = f32[128,1024]{1,0:T(8,128)} fusion(bf16[128,4096]{1,0:T(8,128)(2,1)} %all-gather.3.cloned.1.call-done, bf16[4096,1024]{1,0:T(8,128)(2,1)} %param.11), kind=kOutput, calls=%fused_computation.20 | convolution fusion | flops 1073741824 | bytes 9961472 | tf_op jit(solution)/shard_map/dot_general | solution.py:22
  71.3 0.0 all-reduce.3.cloned.1.call-update
  71.3 0.0 reduce-scatter.5.cloned.1.call-start
  71.4 38.6 %all-reduce.3.cloned.1.call-done = f32[128,1024]{1,0:T(8,128)} async-done(((f32[128,1024]{1,0:T(8,128)}), f32[128,1024]{1,0:T(8,128)}) %all-reduce.3.cloned.1.call-update) | async-done | bytes 524304 | tf_op jit(solution)/shard_map/psum | solution.py:23
  110.0 6.2 %fusion.3 = f32[128,4096]{1,0:T(8,128)} fusion(bf16[1024,4096]{1,0:T(8,128)(2,1)} %param.13, f32[1024]{0:T(1024)S(1)} %copy-done.2, f32[128,1024]{1,0:T(8,128)} %all-reduce.3.cloned.1.call-done, bf16[128,1024]{1,0:T(8,128)(2,1)S(1)} %copy-done), kind=kOutput, calls=%fused_computation.13 | convolution fusion | flops 1074397184 | bytes 11276288 | tf_op jit(solution)/shard_map/dot_general | solution.py:16
  116.2 0.0 reduce-scatter.5.cloned.1.call-update
  116.2 0.0 all-gather.5.cloned.1.call-start
  116.3 0.2 multiply_reduce_fusion.1
  116.5 5.7 %psum.37 = f32[128,1]{0,1:T(1,128)S(1)} all-reduce(f32[128,1]{0,1:T(1,128)S(1)} %bitcast.17), channel_id=1, replica_groups=mesh['grp'=2,'ra'=4,'cb'=4] {'ra'}, use_global_device_ids=true, to_apply=%region_6.7 | all-reduce | flops 128 | bytes 1024 | tf_op jit(solution)/shard_map/psum | solution.py:17
  122.1 25.2 %reduce-scatter.5.cloned.1.call-done = f32[128,1024]{1,0:T(8,128)} async-done(((f32[128,4096]{1,0:T(8,128)}), f32[128,1024]{1,0:T(8,128)}) %reduce-scatter.5.cloned.1.call-update) | async-done | bytes 524304 | tf_op jit(solution)/shard_map/reduce_scatter | solution.py:19
  147.4 1.9 multiply_convert_fusion.1
  149.3 0.0 all-gather.5.cloned.1.call-update
  149.3 0.0 copy-start.3
  149.3 0.0 all-reduce.5.cloned.1.call-start
  149.3 16.8 %all-gather.5.cloned.1.call-done = bf16[128,4096]{1,0:T(8,128)(2,1)} async-done(((bf16[128,1024]{1,0:T(8,128)(2,1)}), bf16[128,4096]{1,0:T(8,128)(2,1)}) %all-gather.5.cloned.1.call-update) | async-done | bytes 1048592 | tf_op jit(solution)/shard_map/all_gather | solution.py:21
  166.1 5.8 %fusion.10 = f32[128,1024]{1,0:T(8,128)} fusion(bf16[128,4096]{1,0:T(8,128)(2,1)} %all-gather.5.cloned.1.call-done, bf16[4096,1024]{1,0:T(8,128)(2,1)} %param.14), kind=kOutput, calls=%fused_computation.21 | convolution fusion | flops 1073741824 | bytes 9961472 | tf_op jit(solution)/shard_map/dot_general | solution.py:22
  171.9 0.0 all-reduce.5.cloned.1.call-update
  172.0 38.8 %all-reduce.5.cloned.1.call-done = f32[128,1024]{1,0:T(8,128)} async-done(((f32[128,1024]{1,0:T(8,128)}), f32[128,1024]{1,0:T(8,128)}) %all-reduce.5.cloned.1.call-update) | async-done | bytes 524304 | tf_op jit(solution)/shard_map/psum | solution.py:23
  210.7 1.2 multiply_reduce_fusion
  212.0 5.7 %psum.39 = f32[128,1]{0,1:T(1,128)S(1)} all-reduce(f32[128,1]{0,1:T(1,128)S(1)} %bitcast.16), channel_id=1, replica_groups=mesh['grp'=2,'ra'=4,'cb'=4] {'ra'}, use_global_device_ids=true, to_apply=%region_9.10 | all-reduce | flops 128 | bytes 1024 | tf_op jit(solution)/shard_map/psum | solution.py:33
  217.6 1.9 multiply_convert_fusion
  (10 shorter events, 0.0 us)
Async XLA Ops:
  6.5 6.2 %copy-start = (bf16[128,1024]{1,0:T(8,128)(2,1)S(1)}, bf16[128,1024]{1,0:T(8,128)(2,1)}, u32[]{:S(2)}) copy-start(bf16[128,1024]{1,0:T(8,128)(2,1)} %param.8) | copy-start | bytes 786436
  6.5 40.3 %reduce-scatter.3.cloned.1.call-start = ((), (), s32[]{:S(2)}) async-start(), calls=%async_computation.2 | async-start | bytes 2621440 | tf_op jit(solution)/shard_map/reduce_scatter | solution.py:19
  12.7 52.8 %all-gather.3.cloned.1.call-start = ((), (), s32[]{:S(2)}) async-start(), calls=%async_computation.3 | async-start | bytes 1310720 | tf_op jit(solution)/shard_map/all_gather | solution.py:21
  48.7 61.3 %copy-start.2 = (f32[1024]{0:T(1024)S(1)}, f32[1024]{0:T(1024)}, u32[]{:S(2)}) copy-start(f32[1024]{0:T(1024)} %param.12) | copy-start | bytes 12292
  48.7 61.3 %all-reduce.3.cloned.1.call-start = ((), (), s32[]{:S(2)}) async-start(), calls=%async_computation.4 | async-start | bytes 1048576 | tf_op jit(solution)/shard_map/psum | solution.py:23
  71.3 76.0 %reduce-scatter.5.cloned.1.call-start = ((), (), s32[]{:S(2)}) async-start(), calls=%async_computation.5 | async-start | bytes 2621440 | tf_op jit(solution)/shard_map/reduce_scatter | solution.py:19
  110.0 6.3 %copy-start.1 = (f32[128,1024]{1,0:T(8,128)S(1)}, f32[128,1024]{1,0:T(8,128)}, u32[]{:S(2)}) copy-start(f32[128,1024]{1,0:T(8,128)} %all-reduce.3.cloned.1.call-done) | copy-start | bytes 1572868
  116.2 49.9 %all-gather.5.cloned.1.call-start = ((), (), s32[]{:S(2)}) async-start(), calls=%async_computation.6 | async-start | bytes 1310720 | tf_op jit(solution)/shard_map/all_gather | solution.py:21
  149.3 68.3 %copy-start.3 = (f32[1024]{0:T(1024)S(1)}, f32[1024]{0:T(1024)}, u32[]{:S(2)}) copy-start(f32[1024]{0:T(1024)} %param.15) | copy-start | bytes 12292
  149.3 61.4 %all-reduce.5.cloned.1.call-start = ((), (), s32[]{:S(2)}) async-start(), calls=%async_computation.7 | async-start | bytes 1048576 | tf_op jit(solution)/shard_map/psum | solution.py:23
Sparse Core Ops, SparseCore 0:
  12.8 33.9 reduce-scatter.2
  48.8 16.6 all-gather.2
  71.5 38.4 all-reduce.2
  116.4 30.9 reduce-scatter.4
  149.4 16.6 all-gather.4
  172.1 38.6 all-reduce.4
where the time goes:
time: 227 us; the launch traced here: 226 us
  waiting for transfers between devices  162 us (71%)
  matrix products  24 us (11%)
  blocking collectives  19.7 us (9%)
  between operations  13.5 us (6%)
  other arithmetic  7.2 us (3%)
    psum x2, waiting for transfers between devices, mlp_block(): branch_out = lax.psum(branch_out, 'cb')  77.4 us
    reduce_scatter x2, waiting for transfers between devices, mlp_block(): lax.psum_scatter(partial_value, 'ra', scatter_dimension=1, tiled=True)  50.7 us
    all_gather x2, waiting for transfers between devices, mlp_block(): hidden = lax.all_gather(activated, 'ra', axis=1, tiled=True)  33.6 us
    psum x2, blocking collectives, mlp_block(): squares_all = lax.psum(squares, 'ra')  14.1 us
    dot_general x2, matrix products, mlp_block(): jnp.dot(normed, up_weight, preferred_element_type=jnp.float32)  12.4 us
    dot_general x2, matrix products, mlp_block(): jnp.dot(hidden, down_weight, preferred_element_type=jnp.float32)  11.6 us
    psum x1, blocking collectives, per_device(): lax.psum(jnp.sum(stream * stream, axis=1, keepdims=True), 'ra')  5.66 us
  transfers between devices with their start and end apart: 6, of which 6 were waited for; matrix products, arithmetic and copies ran while one was open for 0% of the time, Pallas kernels for 0%

commit v1 on v0

v1 whole, which is shorter than its diff:
```python
import functools

import jax
import jax.numpy as jnp
from jax import lax
from jax.experimental import pallas as pl
from jax.experimental.pallas import tpu as pltpu
from jax.sharding import PartitionSpec as P

norm_eps = 1e-06
residual_keep = 0.5
MESH = pl.DeviceIdType.MESH
LANES = 128
HIDDEN_CHUNK = 256
LAG_PAIR = 2
LAG_CHAIN = 3


def kernel(
    R, C,
    tok, gain_1, gain_2, gain_3, up_1, down_1, up_2, down_2,
    out,
    wu, wd, x, stream, own, s_a, r_a, s_b, r_b, act, r_c, acc, s_i, r_i, s_o, r_o, sq_s, sq_r, scale,
    sem_wu, sem_wd, a_send, a_recv, b_send, b_recv, c_send, c_recv,
    i_send, i_recv, o_send, o_recv, q_send, q_recv,
):
    T, width = tok.shape
    chips = R // 2
    NJ, hc = own.shape[0], own.shape[2]
    NP, dc = s_i.shape[1], s_i.shape[3]
    half = NJ * hc
    ups, downs, gains = (up_1, up_2), (down_1, down_2), (gain_1, gain_2, gain_3)

    r = lax.axis_index("ra")
    c = lax.axis_index("cb")
    core = lax.rem(r, 2)
    y = r // 2
    partner = r + 1 - 2 * core
    on_left = c < C // 2
    depth = jnp.where(on_left, c, C - 1 - c)
    inner = jnp.where(on_left, c + 1, c - 1)
    outer = jnp.where(on_left, lax.max(c - 1, 0), lax.min(c + 1, C - 1))
    middle = C // 2 - 1
    lag = lax.min(NP, LAG_CHAIN * (2 * (middle - depth) + 1))

    def load_up(l, side, j):
        at = (core if side == 1 else 1 - core) * half + j * hc
        return pltpu.make_async_copy(
            ups[l].at[:, pl.ds(pl.multiple_of(at, hc), hc)], wu.at[l, side, j], sem_wu.at[l, side, j]
        )

    def load_down(l, side, j):
        at = (core if side == 1 else 1 - core) * half + j * hc
        return pltpu.make_async_copy(
            downs[l].at[pl.ds(pl.multiple_of(at, hc), hc), :], wd.at[l, side, j], sem_wd.at[l, side, j]
        )

    def remote(src, dst, send, recv, axis, to):
        return pltpu.make_async_remote_copy(
            src_ref=src, dst_ref=dst, send_sem=send, recv_sem=recv, device_id={axis: to}, device_id_type=MESH
        )

    def copy_a(l, j):
        return remote(s_a.at[l, j], r_a.at[l, j], a_send.at[l, j], a_recv.at[l, j], "ra", partner)

    def copy_b(l, k, j):
        to = 2 * lax.rem(y + k, chips) + core
        return remote(s_b.at[l, j], r_b.at[l, k - 1, j], b_send.at[l, k - 1, j], b_recv.at[l, k - 1, j], "ra", to)

    def copy_c(l, j):
        return remote(act.at[l, j], r_c.at[l, j], c_send.at[l, j], c_recv.at[l, j], "ra", partner)

    def copy_i(l, p):
        return remote(s_i.at[l, p], r_i.at[l, p], i_send.at[l, p], i_recv.at[l, p], "cb", inner)

    def copy_o(l, p):
        return remote(s_o.at[l, p], r_o.at[l, 1, p], o_send.at[l, 1, p], o_recv.at[l, 1, p], "cb", outer)

    def copy_in(l, p):
        return remote(s_i.at[l, p], r_o.at[l, 0, p], o_send.at[l, 0, p], o_recv.at[l, 0, p], "cb", inner)

    def copy_q(i, k):
        return remote(
            sq_s.at[i], sq_r.at[i, k - 1], q_send.at[i, k - 1], q_recv.at[i, k - 1], "ra", lax.rem(r + k, R)
        )

    def start_squares(i):
        s = stream[...]
        total = jnp.sum(s * s, axis=1, keepdims=True)
        sq_s[i] = jnp.broadcast_to(total, (T, LANES)).T[0:8, :]
        for k in range(1, R):
            copy_q(i, k).start()

    def finish_squares(i):
        total = sq_s[i]
        for k in range(1, R):
            copy_q(i, k).wait_recv()
            total = total + sq_r[i, k - 1]
        factor = lax.rsqrt(total / (width * R) + norm_eps)
        scale[...] = jnp.broadcast_to(factor[0:1, :], (LANES, T)).T

    def columns(p):
        return pl.ds(pl.multiple_of(p * dc, dc), dc)

    @pl.loop(0, NJ)
    def _(j):
        load_up(0, 0, j).start()
        load_up(0, 1, j).start()

    barrier = pltpu.get_barrier_semaphore()
    for k in range(1, R):
        pl.semaphore_signal(barrier, inc=1, device_id={"ra": lax.rem(r + k, R)}, device_id_type=MESH)
    pl.semaphore_signal(barrier, inc=1, device_id={"cb": inner}, device_id_type=MESH)

    @pl.when(depth > 0)
    def _():
        pl.semaphore_signal(barrier, inc=1, device_id={"cb": outer}, device_id_type=MESH)

    stream[...] = tok[...].astype(jnp.float32)
    x[...] = (stream[...] * gain_1[...]).astype(jnp.bfloat16)
    pl.semaphore_wait(barrier, R + jnp.where(depth > 0, 1, 0))

    for l in range(2):
        start_squares(l)

        def reduce_pair(j):
            copy_a(l, j).wait_recv()
            both = own[j] + r_a[l, j].astype(jnp.float32)
            own[j] = both
            s_b[l, j] = both.astype(jnp.bfloat16)
            for k in range(1, chips):
                copy_b(l, k, j).start()

        @pl.loop(0, NJ)
        def _(j):
            load_up(l, 0, j).wait()
            s_a[l, j] = jnp.dot(x[...], wu[l, 0, j], preferred_element_type=jnp.float32).astype(jnp.bfloat16)
            copy_a(l, j).start()
            load_up(l, 1, j).wait()
            own[j] = jnp.dot(x[...], wu[l, 1, j], preferred_element_type=jnp.float32)
            load_down(l, 1, j).start()
            load_down(l, 0, j).start()

            @pl.when(j >= LAG_PAIR)
            def _():
                reduce_pair(j - LAG_PAIR)

        @pl.loop(max(NJ - LAG_PAIR, 0), NJ)
        def _(j):
            reduce_pair(j)

        finish_squares(l)
        acc[...] = jnp.zeros_like(acc)

        def add_other(j):
            copy_c(l, j).wait_recv()
            load_down(l, 0, j).wait()
            acc[...] += jnp.dot(r_c[l, j], wd[l, 0, j], preferred_element_type=jnp.float32)

        @pl.loop(0, NJ)
        def _(j):
            total = own[j]
            for k in range(1, chips):
                copy_b(l, k, j).wait_recv()
                total = total + r_b[l, k - 1, j].astype(jnp.float32)
            pre = total * scale[:, 0:1]
            act[l, j] = jnp.square(jnp.maximum(pre, 0.0)).astype(jnp.bfloat16)
            copy_c(l, j).start()
            if l == 0:
                load_up(1, 0, j).start()
                load_up(1, 1, j).start()
            load_down(l, 1, j).wait()
            acc[...] += jnp.dot(act[l, j], wd[l, 1, j], preferred_element_type=jnp.float32)

            @pl.when(j >= 1)
            def _():
                add_other(j - 1)

        add_other(NJ - 1)

        def send_inward(p):
            @pl.when(depth > 0)
            def _():
                copy_in(l, p).wait_recv()
                acc[:, columns(p)] += r_o[l, 0, p].astype(jnp.float32)

            s_i[l, p] = acc[:, columns(p)].astype(jnp.bfloat16)

            @pl.when(depth == middle)
            def _():
                copy_i(l, p).start()

            @pl.when(depth < middle)
            def _():
                copy_in(l, p).start()

        def send_outward(p):
            @pl.when(depth == middle)
            def _():
                copy_i(l, p).wait_recv()
                total = s_i[l, p].astype(jnp.float32) + r_i[l, p].astype(jnp.float32)
                s_o[l, p] = total.astype(jnp.bfloat16)

                if middle > 0:
                    copy_o(l, p).start()

                stream[:, columns(p)] = residual_keep * stream[:, columns(p)] + s_o[l, p].astype(jnp.float32)

            if middle > 0:
                @pl.when(depth < middle)
                def _():
                    copy_o(l, p).wait_recv()

                    @pl.when(depth > 0)
                    def _():
                        s_o[l, p] = r_o[l, 1, p]
                        copy_o(l, p).start()

                    stream[:, columns(p)] = (
                        residual_keep * stream[:, columns(p)] + r_o[l, 1, p].astype(jnp.float32)
                    )

            if l == 0:
                x[:, columns(p)] = (stream[:, columns(p)] * gain_2[:, columns(p)]).astype(jnp.bfloat16)

        @pl.loop(0, 2 * NP)
        def _(step):
            @pl.when(step < NP)
            def _():
                send_inward(step)

            @pl.when(jnp.logical_and(step >= lag, step < lag + NP))
            def _():
                send_outward(step - lag)

    start_squares(2)
    finish_squares(2)
    out[...] = (stream[...] * scale[:, 0:1] * gain_3[...]).astype(out.dtype)

    for l in range(2):
        @pl.loop(0, NJ)
        def _(j):
            copy_a(l, j).wait_send()
            for k in range(1, chips):
                copy_b(l, k, j).wait_send()
            copy_c(l, j).wait_send()

        @pl.loop(0, NP)
        def _(p):
            @pl.when(depth == middle)
            def _():
                copy_i(l, p).wait_send()

            @pl.when(depth < middle)
            def _():
                copy_in(l, p).wait_send()

            @pl.when(depth > 0)
            def _():
                copy_o(l, p).wait_send()

    for i in range(3):
        for k in range(1, R):
            copy_q(i, k).wait_send()


def per_device(R, C, tokens, gain_1, up_1, down_1, gain_2, up_2, down_2, gain_3):
    T, width = tokens.shape
    hidden = up_1.shape[1]
    chips = R // 2
    hc = min(HIDDEN_CHUNK, hidden // 2)
    NJ = hidden // 2 // hc
    dc = LANES
    NP = width // dc
    bf16, f32 = jnp.bfloat16, jnp.float32
    dma = pltpu.SemaphoreType.DMA
    others = max(chips - 1, 1)
    scratch = [
        pltpu.VMEM((2, 2, NJ, width, hc), bf16),
        pltpu.VMEM((2, 2, NJ, hc, width), bf16),
        pltpu.VMEM((T, width), bf16),
        pltpu.VMEM((T, width), f32),
        pltpu.VMEM((NJ, T, hc), f32),
        pltpu.VMEM((2, NJ, T, hc), bf16),
        pltpu.VMEM((2, NJ, T, hc), bf16),
        pltpu.VMEM((2, NJ, T, hc), bf16),
        pltpu.VMEM((2, others, NJ, T, hc), bf16),
        pltpu.VMEM((2, NJ, T, hc), bf16),
        pltpu.VMEM((2, NJ, T, hc), bf16),
        pltpu.VMEM((T, width), f32),
        pltpu.VMEM((2, NP, T, dc), bf16),
        pltpu.VMEM((2, NP, T, dc), bf16),
        pltpu.VMEM((2, NP, T, dc), bf16),
        pltpu.VMEM((2, 2, NP, T, dc), bf16),
        pltpu.VMEM((3, 8, T), f32),
        pltpu.VMEM((3, R - 1, 8, T), f32),
        pltpu.VMEM((T, LANES), f32),
        dma((2, 2, NJ)), dma((2, 2, NJ)),
        dma((2, NJ)), dma((2, NJ)),
        dma((2, others, NJ)), dma((2, others, NJ)),
        dma((2, NJ)), dma((2, NJ)),
        dma((2, NP)), dma((2, NP)),
        dma((2, 2, NP)), dma((2, 2, NP)),
        dma((3, R - 1)), dma((3, R - 1)),
    ]
    vmem, hbm = pl.BlockSpec(memory_space=pltpu.VMEM), pl.BlockSpec(memory_space=pl.ANY)
    return pl.pallas_call(
        functools.partial(kernel, R, C),
        out_shape=jax.ShapeDtypeStruct((T, width), bf16),
        in_specs=[vmem] * 4 + [hbm] * 4,
        out_specs=vmem,
        scratch_shapes=scratch,
        compiler_params=pltpu.CompilerParams(
            collective_id=0, has_side_effects=True, vmem_limit_bytes=60 * 1024 * 1024
        ),
    )(
        tokens, gain_1.reshape(1, width), gain_2.reshape(1, width), gain_3.reshape(1, width),
        up_1, down_1, up_2, down_2,
    )


def solution(mesh):
    in_specs = (
        P("grp", "ra"),
        P("ra"),
        P("ra", "cb"),
        P("cb", "ra"),
        P("ra"),
        P("ra", "cb"),
        P("cb", "ra"),
        P("ra"),
    )
    return jax.shard_map(
        functools.partial(per_device, mesh.shape["ra"], mesh.shape["cb"]),
        mesh=mesh, in_specs=in_specs, out_specs=P("grp", "ra"), check_vma=False,
    )
```

time: 227 us -> 73.1 us (0.32)
  waiting for transfers between devices: 162 us -> 0 us
  Pallas kernels: 0 us -> 71.3 us
  matrix products: 24 us -> 0 us
  blocking collectives: 19.7 us -> 0 us
  between operations: 13.5 us -> 0.01 us
  other arithmetic: 7.2 us -> 0 us
    psum x2 -> x0, waiting for transfers between devices: 77.4 us -> none  [mlp_block(): branch_out = lax.psum(branch_out, 'cb')]
    pallas_call x0 -> x1, Pallas kernels: none -> 71.3 us  [per_device(): pl.pallas_call(functools.partial(kernel, R, C), out_shape=jax.ShapeDtypeS...]
    reduce_scatter x2 -> x0, waiting for transfers between devices: 50.7 us -> none  [mlp_block(): lax.psum_scatter(partial_value, 'ra', scatter_dimension=1, tiled=True)]
    all_gather x2 -> x0, waiting for transfers between devices: 33.6 us -> none  [mlp_block(): hidden = lax.all_gather(activated, 'ra', axis=1, tiled=True)]
    dot_general x4 -> x0, matrix products: 24 us -> none  [the longest x2 12.4 us: mlp_block(): jnp.dot(normed, up_weight, preferred_element_type=jnp.float32)]
    psum x3 -> x0, blocking collectives: 19.7 us -> none  [the longest x2 14.1 us: mlp_block(): squares_all = lax.psum(squares, 'ra')]
    convert_element_type x3 -> x0, other arithmetic: 5.63 us -> none  [the longest x2 3.74 us: mlp_block(): activated = jnp.square(jax.nn.relu(share * row_scale)).astype(jnp.bfloat16)]
  transfers between devices with their start and end apart: 6 -> 0, of which waited for: 6 -> 0; matrix products, arithmetic and copies ran while one was open for 0% -> 0% of each run, Pallas kernels for 0% -> 0%
where the time goes in v1:
time: 73.1 us; the launch traced here: 73 us
  Pallas kernels  71.3 us (98%)
  local copies, waits for them, and re-layouts  1.67 us (2%)
    pallas_call x1, Pallas kernels, per_device(): pl.pallas_call(functools.partial(kernel, R, C), out_shape=jax.ShapeDtypeS...  71.3 us
    unnamed x1, local copies, waits for them, and re-layouts  1.67 us

profile of v1, /device:TPU:0, one launch (start us, length us, event | category | flops | bytes accessed | tf_op | source)
XLA Modules:
  0.0 73.0 jit_solution(14528351295841475550)
XLA Ops:
  0.0 71.3 %shard_map.82 = bf16[128,1024]{1,0:T(8,128)(2,1)} custom-call(bf16[128,1024]{1,0:T(8,128)(2,1)} %tok.1, f32[1,1024]{1,0:T(1,128)} %bitcast.3, f32[1,1024]{1,0:T(1,128)} %bitcast.4, f32[1,1024]{1,0:T(1,128)} %bitcast.5, bf16[1024,4096]{1,0:T(8,128)(2,1)} %up_1.1, bf16[4096,1024]{1,0:T(8,128)(2,1)} %down_1.1, bf16[1024,4096]{1,0:T(8,128)(2,1)} %up_2.1, ...), custom_call_target="tpu_custom_call" | custom-call | tf_op jit(solution)/shard_map/pallas_call | solution.py:307
  71.3 1.7 %copy.10 = bf16[128,1024]{1,0:T(8,128)(2,1)} copy(bf16[128,1024]{1,0:T(8,128)(2,1)} %shard_map.82) | data formatting | bytes 524288

commit v2 on v1

v2 whole, which is shorter than its diff:
```python
import functools

import jax
import jax.numpy as jnp
from jax import lax
from jax.experimental import pallas as pl
from jax.experimental.pallas import tpu as pltpu
from jax.sharding import PartitionSpec as P

norm_eps = 1e-06
residual_keep = 0.5
MESH = pl.DeviceIdType.MESH
LANES = 128
HIDDEN_CHUNK = 512
LAG_PAIR = 2
SKIP = 2
CHAIN_CHUNK = 256


def kernel(
    R, C,
    tok, gain_1, gain_2, gain_3, up_1, down_1, up_2, down_2,
    out,
    wu, wd, x, stream, own, s_a, r_a, s_b, r_b, act, r_c, acc, s_i, r_i, s_o, r_o, sq_s, sq_r, scale,
    sem_wu, sem_wd, a_send, a_recv, b_send, b_recv, c_send, c_recv,
    i_send, i_recv, o_send, o_recv, q_send, q_recv,
):
    T, width = tok.shape
    chips = R // 2
    NJ, hc = own.shape[1], own.shape[3]
    NP, dc = s_i.shape[1], s_i.shape[3]
    half = NJ * hc
    ups, downs, gains = (up_1, up_2), (down_1, down_2), (gain_1, gain_2, gain_3)

    r = lax.axis_index("ra")
    c = lax.axis_index("cb")
    core = lax.rem(r, 2)
    y = r // 2
    partner = r + 1 - 2 * core
    on_left = c < C // 2
    depth = jnp.where(on_left, c, C - 1 - c)
    inner = jnp.where(on_left, c + 1, c - 1)
    outer = jnp.where(on_left, lax.max(c - 1, 0), lax.min(c + 1, C - 1))
    middle = C // 2 - 1
    half_T = T // 2

    def load_up(l, side, j):
        at = (core if side == 1 else 1 - core) * half + j * hc
        return pltpu.make_async_copy(
            ups[l].at[:, pl.ds(pl.multiple_of(at, hc), hc)], wu.at[l, side, j], sem_wu.at[l, side, j]
        )

    def load_down(l, side, j):
        at = (core if side == 1 else 1 - core) * half + j * hc
        return pltpu.make_async_copy(
            downs[l].at[pl.ds(pl.multiple_of(at, hc), hc), :], wd.at[l, side, j], sem_wd.at[l, side, j]
        )

    def remote(src, dst, send, recv, axis, to):
        return pltpu.make_async_remote_copy(
            src_ref=src, dst_ref=dst, send_sem=send, recv_sem=recv, device_id={axis: to}, device_id_type=MESH
        )

    def rows(h):
        return pl.ds(h * half_T, half_T)

    def copy_a(s, j):
        return remote(s_a.at[s, j], r_a.at[s, j], a_send.at[s, j], a_recv.at[s, j], "ra", partner)

    def copy_b(s, k, j):
        to = 2 * lax.rem(y + k, chips) + core
        return remote(s_b.at[s, j], r_b.at[s, k - 1, j], b_send.at[s, k - 1, j], b_recv.at[s, k - 1, j], "ra", to)

    def copy_c(s, j):
        return remote(act.at[s, j], r_c.at[s, j], c_send.at[s, j], c_recv.at[s, j], "ra", partner)

    def copy_i(s, p):
        return remote(s_i.at[s, p], r_i.at[s, p], i_send.at[s, p], i_recv.at[s, p], "cb", inner)

    def copy_o(s, p):
        return remote(s_o.at[s, p], r_o.at[s, 1, p], o_send.at[s, 1, p], o_recv.at[s, 1, p], "cb", outer)

    def copy_in(s, p):
        return remote(s_i.at[s, p], r_o.at[s, 0, p], o_send.at[s, 0, p], o_recv.at[s, 0, p], "cb", inner)

    def copy_q(i, k):
        return remote(
            sq_s.at[i], sq_r.at[i, k - 1], q_send.at[i, k - 1], q_recv.at[i, k - 1], "ra", lax.rem(r + k, R)
        )

    def start_squares(i, halves):
        parts = []
        for h in halves:
            s = stream[rows(h), :]
            total = jnp.sum(s * s, axis=1, keepdims=True)
            parts.append(jnp.broadcast_to(total, (half_T, LANES)))
        if len(parts) == 1:
            parts = parts * 2
        sq_s[i] = jnp.concatenate(parts, axis=0).T[0:8, :]
        for k in range(1, R):
            copy_q(i, k).start()

    def finish_squares(i, halves):
        total = sq_s[i]
        for k in range(1, R):
            copy_q(i, k).wait_recv()
            total = total + sq_r[i, k - 1]
        factor = lax.rsqrt(total / (width * R) + norm_eps)
        spread = jnp.broadcast_to(factor[0:1, :], (LANES, T)).T
        for h in halves:
            scale[rows(h), :] = spread[h * half_T:(h + 1) * half_T, :]

    def columns(p):
        return pl.ds(pl.multiple_of(p * dc, dc), dc)

    def reduce_pair(s, h, j):
        copy_a(s, j).wait_recv()
        both = own[h, j] + r_a[s, j].astype(jnp.float32)
        own[h, j] = both
        s_b[s, j] = both.astype(jnp.bfloat16)
        for k in range(1, chips):
            copy_b(s, k, j).start()

    def up(l, h, hook=None):
        s = 2 * l + h

        @pl.loop(0, NJ)
        def _(j):
            if h == 0:
                load_up(l, 0, j).wait()
            s_a[s, j] = jnp.dot(
                x[rows(h), :], wu[l, 0, j], preferred_element_type=jnp.float32
            ).astype(jnp.bfloat16)
            copy_a(s, j).start()
            if h == 0:
                load_up(l, 1, j).wait()
            own[h, j] = jnp.dot(x[rows(h), :], wu[l, 1, j], preferred_element_type=jnp.float32)
            if h == 0:
                load_down(l, 1, j).start()
                load_down(l, 0, j).start()

            @pl.when(j >= LAG_PAIR)
            def _():
                reduce_pair(s, h, j - LAG_PAIR)

            if hook is not None:
                hook(j)

        @pl.loop(max(NJ - LAG_PAIR, 0), NJ)
        def _(j):
            reduce_pair(s, h, j)

    def down(l, h, hook=None):
        s = 2 * l + h
        acc[h] = jnp.zeros((half_T, width), jnp.float32)

        def add_other(j):
            copy_c(s, j).wait_recv()
            if h == 0:
                load_down(l, 0, j).wait()
            acc[h] += jnp.dot(r_c[s, j], wd[l, 0, j], preferred_element_type=jnp.float32)

        @pl.loop(0, NJ)
        def _(j):
            total = own[h, j]
            for k in range(1, chips):
                copy_b(s, k, j).wait_recv()
                total = total + r_b[s, k - 1, j].astype(jnp.float32)
            pre = total * scale[rows(h), 0:1]
            act[s, j] = jnp.square(jnp.maximum(pre, 0.0)).astype(jnp.bfloat16)
            copy_c(s, j).start()
            if h == 0:
                if l == 0:
                    load_up(1, 0, j).start()
                    load_up(1, 1, j).start()
                load_down(l, 1, j).wait()
            acc[h] += jnp.dot(act[s, j], wd[l, 1, j], preferred_element_type=jnp.float32)

            @pl.when(j >= 1)
            def _():
                add_other(j - 1)

            if hook is not None:
                hook(j)

        add_other(NJ - 1)

    def send_inward(l, h, p):
        s = 2 * l + h

        @pl.when(depth > 0)
        def _():
            copy_in(s, p).wait_recv()
            acc[h, :, columns(p)] += r_o[s, 0, p].astype(jnp.float32)

        s_i[s, p] = acc[h, :, columns(p)].astype(jnp.bfloat16)

        @pl.when(depth == middle)
        def _():
            copy_i(s, p).start()

        @pl.when(depth < middle)
        def _():
            copy_in(s, p).start()

    def send_outward(l, h, p):
        s = 2 * l + h

        def add(branch):
            stream[rows(h), columns(p)] = residual_keep * stream[rows(h), columns(p)] + branch.astype(jnp.float32)

        @pl.when(depth == middle)
        def _():
            copy_i(s, p).wait_recv()
            total = s_i[s, p].astype(jnp.float32) + r_i[s, p].astype(jnp.float32)
            s_o[s, p] = total.astype(jnp.bfloat16)
            if middle > 0:
                copy_o(s, p).start()
            add(s_o[s, p])

        if middle > 0:
            @pl.when(depth < middle)
            def _():
                copy_o(s, p).wait_recv()

                @pl.when(depth > 0)
                def _():
                    s_o[s, p] = r_o[s, 1, p]
                    copy_o(s, p).start()

                add(r_o[s, 1, p])

        if l == 0:
            x[rows(h), columns(p)] = (stream[rows(h), columns(p)] * gain_2[:, columns(p)]).astype(jnp.bfloat16)

    def inward_if(inside, l, h, first, last):
        @pl.when((depth == middle) if inside else (depth < middle))
        def _():
            @pl.loop(first, last)
            def _(p):
                send_inward(l, h, p)

    def outward(l, h):
        @pl.loop(0, NP)
        def _(p):
            send_outward(l, h, p)

    @pl.loop(0, NJ)
    def _(j):
        load_up(0, 0, j).start()
        load_up(0, 1, j).start()

    barrier = pltpu.get_barrier_semaphore()
    for k in range(1, R):
        pl.semaphore_signal(barrier, inc=1, device_id={"ra": lax.rem(r + k, R)}, device_id_type=MESH)
    pl.semaphore_signal(barrier, inc=1, device_id={"cb": inner}, device_id_type=MESH)

    @pl.when(depth > 0)
    def _():
        pl.semaphore_signal(barrier, inc=1, device_id={"cb": outer}, device_id_type=MESH)

    stream[...] = tok[...].astype(jnp.float32)
    x[...] = (stream[...] * gain_1[...]).astype(jnp.bfloat16)
    pl.semaphore_wait(barrier, R + jnp.where(depth > 0, 1, 0))

    start_squares(0, (0, 1))
    up(0, 0)
    up(0, 1)
    finish_squares(0, (0, 1))

    for l in range(2):
        if l == 1:
            finish_squares(1, (0,))
        down(l, 0)
        inward_if(False, l, 0, 0, NP)
        if l == 1:
            finish_squares(2, (1,))

        def in_down(j):
            @pl.when(jnp.logical_and(depth == middle, jnp.logical_and(j >= SKIP, j < NP + SKIP)))
            def _():
                send_inward(l, 0, j - SKIP)

        down(l, 1, in_down)
        inward_if(False, l, 1, 0, NP)
        inward_if(True, l, 0, min(NP, max(NJ - SKIP, 0)), NP)
        outward(l, 0)
        if l == 0:
            start_squares(1, (0,))

            def in_up(j):
                @pl.when(jnp.logical_and(depth == middle, j < NP))
                def _():
                    send_inward(0, 1, j)

            up(1, 0, in_up)
            inward_if(True, l, 1, min(NJ, NP), NP)
            outward(l, 1)
            start_squares(2, (1,))
            up(1, 1)
        else:
            start_squares(3, (0,))
            inward_if(True, l, 1, 0, NP)
            outward(l, 1)
            start_squares(4, (1,))

    finish_squares(3, (0,))
    finish_squares(4, (1,))
    out[...] = (stream[...] * scale[:, 0:1] * gain_3[...]).astype(out.dtype)

    for s in range(4):
        @pl.loop(0, NJ)
        def _(j):
            copy_a(s, j).wait_send()
            for k in range(1, chips):
                copy_b(s, k, j).wait_send()
            copy_c(s, j).wait_send()

        @pl.loop(0, NP)
        def _(p):
            @pl.when(depth == middle)
            def _():
                copy_i(s, p).wait_send()

            @pl.when(depth < middle)
            def _():
                copy_in(s, p).wait_send()

            @pl.when(depth > 0)
            def _():
                copy_o(s, p).wait_send()

    for i in range(5):
        for k in range(1, R):
            copy_q(i, k).wait_send()


def per_device(R, C, tokens, gain_1, up_1, down_1, gain_2, up_2, down_2, gain_3):
    T, width = tokens.shape
    hidden = up_1.shape[1]
    chips = R // 2
    hc = min(HIDDEN_CHUNK, hidden // 2)
    NJ = hidden // 2 // hc
    half_T = T // 2
    dc = min(CHAIN_CHUNK, width)
    NP = width // dc
    bf16, f32 = jnp.bfloat16, jnp.float32
    dma = pltpu.SemaphoreType.DMA
    others = max(chips - 1, 1)
    scratch = [
        pltpu.VMEM((2, 2, NJ, width, hc), bf16),
        pltpu.VMEM((2, 2, NJ, hc, width), bf16),
        pltpu.VMEM((T, width), bf16),
        pltpu.VMEM((T, width), f32),
        pltpu.VMEM((2, NJ, half_T, hc), f32),
        pltpu.VMEM((4, NJ, half_T, hc), bf16),
        pltpu.VMEM((4, NJ, half_T, hc), bf16),
        pltpu.VMEM((4, NJ, half_T, hc), bf16),
        pltpu.VMEM((4, others, NJ, half_T, hc), bf16),
        pltpu.VMEM((4, NJ, half_T, hc), bf16),
        pltpu.VMEM((4, NJ, half_T, hc), bf16),
        pltpu.VMEM((2, half_T, width), f32),
        pltpu.VMEM((4, NP, half_T, dc), bf16),
        pltpu.VMEM((4, NP, half_T, dc), bf16),
        pltpu.VMEM((4, NP, half_T, dc), bf16),
        pltpu.VMEM((4, 2, NP, half_T, dc), bf16),
        pltpu.VMEM((5, 8, T), f32),
        pltpu.VMEM((5, R - 1, 8, T), f32),
        pltpu.VMEM((T, LANES), f32),
        dma((2, 2, NJ)), dma((2, 2, NJ)),
        dma((4, NJ)), dma((4, NJ)),
        dma((4, others, NJ)), dma((4, others, NJ)),
        dma((4, NJ)), dma((4, NJ)),
        dma((4, NP)), dma((4, NP)),
        dma((4, 2, NP)), dma((4, 2, NP)),
        dma((5, R - 1)), dma((5, R - 1)),
    ]
    vmem, hbm = pl.BlockSpec(memory_space=pltpu.VMEM), pl.BlockSpec(memory_space=pl.ANY)
    return pl.pallas_call(
        functools.partial(kernel, R, C),
        out_shape=jax.ShapeDtypeStruct((T, width), bf16),
        in_specs=[vmem] * 4 + [hbm] * 4,
        out_specs=vmem,
        scratch_shapes=scratch,
        compiler_params=pltpu.CompilerParams(
            collective_id=0, has_side_effects=True, vmem_limit_bytes=60 * 1024 * 1024
        ),
    )(
        tokens, gain_1.reshape(1, width), gain_2.reshape(1, width), gain_3.reshape(1, width),
        up_1, down_1, up_2, down_2,
    )


def solution(mesh):
    in_specs = (
        P("grp", "ra"),
        P("ra"),
        P("ra", "cb"),
        P("cb", "ra"),
        P("ra"),
        P("ra", "cb"),
        P("cb", "ra"),
        P("ra"),
    )
    return jax.shard_map(
        functools.partial(per_device, mesh.shape["ra"], mesh.shape["cb"]),
        mesh=mesh, in_specs=in_specs, out_specs=P("grp", "ra"), check_vma=False,
    )
```

time: 73.1 us -> 64.2 us (0.88)
  Pallas kernels: 71.3 us -> 62.3 us
    pallas_call x1, Pallas kernels: 71.3 us -> 62.3 us  [per_device(): pl.pallas_call(functools.partial(kernel, R, C), out_shape=jax.ShapeDtypeS...]
where the time goes in v2:
time: 64.2 us; the launch traced here: 64 us
  Pallas kernels  62.3 us (97%)
  local copies, waits for them, and re-layouts  1.67 us (3%)
    pallas_call x1, Pallas kernels, per_device(): pl.pallas_call(functools.partial(kernel, R, C), out_shape=jax.ShapeDtypeS...  62.3 us
    unnamed x1, local copies, waits for them, and re-layouts  1.67 us

profile of v2, /device:TPU:0, one launch (start us, length us, event | category | flops | bytes accessed | tf_op | source)
XLA Modules:
  0.0 64.0 jit_solution(1104899284955594818)
XLA Ops:
  0.0 62.3 %shard_map.82 = bf16[128,1024]{1,0:T(8,128)(2,1)} custom-call(bf16[128,1024]{1,0:T(8,128)(2,1)} %tok.1, f32[1,1024]{1,0:T(1,128)} %bitcast.3, f32[1,1024]{1,0:T(1,128)} %bitcast.4, f32[1,1024]{1,0:T(1,128)} %bitcast.5, bf16[1024,4096]{1,0:T(8,128)(2,1)} %up_1.1, bf16[4096,1024]{1,0:T(8,128)(2,1)} %down_1.1, bf16[1024,4096]{1,0:T(8,128)(2,1)} %up_2.1, ...), custom_call_target="tpu_custom_call" | custom-call | tf_op jit(solution)/shard_map/pallas_call | solution.py:379
  62.4 1.7 %copy.10 = bf16[128,1024]{1,0:T(8,128)(2,1)} copy(bf16[128,1024]{1,0:T(8,128)(2,1)} %shard_map.82) | data formatting | bytes 524288

commit v3 on v2

--- a/solution.py
+++ b/solution.py
@@ -12,9 +12,9 @@
 MESH = pl.DeviceIdType.MESH
 LANES = 128
 HIDDEN_CHUNK = 512
-LAG_PAIR = 2
+LAG_PAIR = 1
 SKIP = 2
-CHAIN_CHUNK = 256
+CHAIN_CHUNK = 512
 
 
 def kernel(
@@ -47,7 +47,7 @@
     def load_up(l, side, j):
         at = (core if side == 1 else 1 - core) * half + j * hc
         return pltpu.make_async_copy(
-            ups[l].at[:, pl.ds(pl.multiple_of(at, hc), hc)], wu.at[l, side, j], sem_wu.at[l, side, j]
+            ups[l].at[:, pl.ds(pl.multiple_of(at, hc), hc)], wu.at[l, j, :, pl.ds(side * hc, hc)], sem_wu.at[l, side, j]
         )
 
     def load_down(l, side, j):
@@ -128,13 +128,11 @@
         def _(j):
             if h == 0:
                 load_up(l, 0, j).wait()
-            s_a[s, j] = jnp.dot(
-                x[rows(h), :], wu[l, 0, j], preferred_element_type=jnp.float32
-            ).astype(jnp.bfloat16)
+                load_up(l, 1, j).wait()
+            sides = jnp.dot(x[rows(h), :], wu[l, j], preferred_element_type=jnp.float32)
+            s_a[s, j] = sides[:, :hc].astype(jnp.bfloat16)
             copy_a(s, j).start()
-            if h == 0:
-                load_up(l, 1, j).wait()
-            own[h, j] = jnp.dot(x[rows(h), :], wu[l, 1, j], preferred_element_type=jnp.float32)
+            own[h, j] = sides[:, hc:]
             if h == 0:
                 load_down(l, 1, j).start()
                 load_down(l, 0, j).start()
@@ -348,7 +346,7 @@
     dma = pltpu.SemaphoreType.DMA
     others = max(chips - 1, 1)
     scratch = [
-        pltpu.VMEM((2, 2, NJ, width, hc), bf16),
+        pltpu.VMEM((2, NJ, width, 2 * hc), bf16),
         pltpu.VMEM((2, 2, NJ, hc, width), bf16),
         pltpu.VMEM((T, width), bf16),
         pltpu.VMEM((T, width), f32),

time: 64.2 us -> 64.5 us (level)
  no operation moved by 1% of the time
where the time goes in v3:
time: 64.5 us; the launch traced here: 64.3 us
  Pallas kernels  62.6 us (97%)
  local copies, waits for them, and re-layouts  1.67 us (3%)
    pallas_call x1, Pallas kernels, per_device(): pl.pallas_call(functools.partial(kernel, R, C), out_shape=jax.ShapeDtypeS...  62.6 us
    unnamed x1, local copies, waits for them, and re-layouts  1.67 us

profile of v3, /device:TPU:0, one launch (start us, length us, event | category | flops | bytes accessed | tf_op | source)
XLA Modules:
  0.0 64.3 jit_solution(7929660415295382999)
XLA Ops:
  0.0 62.6 %shard_map.82 = bf16[128,1024]{1,0:T(8,128)(2,1)} custom-call(bf16[128,1024]{1,0:T(8,128)(2,1)} %tok.1, f32[1,1024]{1,0:T(1,128)} %bitcast.3, f32[1,1024]{1,0:T(1,128)} %bitcast.4, f32[1,1024]{1,0:T(1,128)} %bitcast.5, bf16[1024,4096]{1,0:T(8,128)(2,1)} %up_1.1, bf16[4096,1024]{1,0:T(8,128)(2,1)} %down_1.1, bf16[1024,4096]{1,0:T(8,128)(2,1)} %up_2.1, ...), custom_call_target="tpu_custom_call" | custom-call | tf_op jit(solution)/shard_map/pallas_call | solution.py:377
  62.7 1.7 %copy.10 = bf16[128,1024]{1,0:T(8,128)(2,1)} copy(bf16[128,1024]{1,0:T(8,128)(2,1)} %shard_map.82) | data formatting | bytes 524288
